TPU v7x, 32 devices: a whole 2x2x4 slice. The times are simulated.
32 devices in a mesh: fs: 16 (over z, y, x), tp: 2 (over core).
Axes of the slice: x: 2, y: 2, z: 4, core: 2. Of those that a mesh axis runs over, the one named last changes fastest.
Arguments:
- normed_input: bfloat16 [8192, 4096], P('fs', 'tp'), may hold values from -6 to 6
- value_cotangent: bfloat16 [8192, 2048], P('fs', 'tp'), may hold values from -0.01171875 to 0.01171875
- mixer_output: bfloat16 [8192, 2048], P('fs', 'tp'), may hold values from -6 to 6
- output_cotangent: bfloat16 [8192, 4096], P('fs', 'tp'), may hold values from -0.015625 to 0.015625
- value_factor: bfloat16 [4096, 128], replicated, may hold values from -0.5 to 0.5
- output_factor: bfloat16 [2048, 128], replicated, may hold values from -0.5 to 0.5
- value_master: float32 [4096, 2048], P('fs', 'tp'), may hold values from -0.09375 to 0.09375
- value_moment: float32 [128, 2048], P(None, 'tp'), may hold values from -6 to 6
- value_second: float32 [128, 2048], P(None, 'tp'), may hold values from 0.0625 to 16, as said below
- output_master: float32 [2048, 4096], P('fs', 'tp'), may hold values from -0.125 to 0.125
- output_moment: float32 [128, 4096], P(None, 'tp'), may hold values from -6 to 6
- output_second: float32 [128, 4096], P(None, 'tp'), may hold values from 0.0625 to 16, as said below
Outputs:
- value_step: float32 [4096, 2048], P('fs', 'tp')
- value_new: float32 [4096, 2048], P('fs', 'tp')
- value_copy: bfloat16 [4096, 2048], P(None, 'tp')
- value_moment_new: float32 [128, 2048], P(None, 'tp')
- value_second_new: float32 [128, 2048], P(None, 'tp')
- output_step: float32 [2048, 4096], P('fs', 'tp')
- output_new: float32 [2048, 4096], P('fs', 'tp')
- output_copy: bfloat16 [2048, 4096], P(None, 'tp')
- output_moment_new: float32 [128, 4096], P(None, 'tp')
- output_second_new: float32 [128, 4096], P(None, 'tp')
Inputs may be any that keep to these rules, and one draw needn't show every extreme that they name: `value_second`: positive, with a scale that differs between groups of columns. `output_second`: positive, with a scale that differs between groups of columns.
All inputs are finite; a program needn't handle non-finite values.
Results may differ from a plain program's by a relative error of at most 0.004.
Values may be sent and summed in bfloat16 or wider, within the bound.
A program may use at most 128 MiB of HBM per device.

v0:
```python
import functools

import jax
import jax.numpy as jnp
from jax import lax
from jax.experimental import pallas as pl
from jax.experimental.pallas import tpu as pltpu
from jax.sharding import PartitionSpec as P

BETA_ONE = 0.8
BETA_TWO = 0.9
EPSILON = 1e-08
STEP_RATE = 0.005
FLOOR = 0.25

MESH = pl.DeviceIdType.MESH
PIECES = 8
UP, DOWN, ACROSS_A, ACROSS_B = range(4)
GROUPS = (
    (0, 0, 4, True, (ACROSS_A, ACROSS_B)),
    (1, 0, 4, True, (ACROSS_B, ACROSS_A)),
    (0, 4, 7, True, (ACROSS_B, ACROSS_A)),
    (1, 4, 7, True, (ACROSS_A, ACROSS_B)),
    (0, 7, 8, False, (ACROSS_A, ACROSS_B)),
    (1, 7, 8, False, (ACROSS_B, ACROSS_A)),
    (2, None, None, True, (ACROSS_A, ACROSS_B)),
    (3, None, None, True, (ACROSS_B, ACROSS_A)),
)


def transfer_kernel(
    n_fs,
    n_tp,
    normed_hbm,
    mixer_hbm,
    value_cot_hbm,
    output_cot_hbm,
    value_factor_hbm,
    output_factor_hbm,
    value_moment_hbm,
    value_second_hbm,
    output_moment_hbm,
    output_second_hbm,
    value_master,
    output_master,
    value_all,
    output_all,
    value_sum,
    output_sum,
    value_high,
    value_low,
    output_high,
    output_low,
    scales,
    normed,
    mixer,
    value_cot_ref,
    output_cot_ref,
    value_factor,
    output_factor,
    value_moment,
    value_second,
    output_moment,
    output_second,
    load_sem,
    value_own,
    output_own,
    input_ref,
    mixer_ref,
    near_in,
    near_mix,
    squares,
    near_squares,
    value_part,
    output_part,
    value_recv,
    output_recv,
    gather_send,
    gather_recv,
    local_sem,
    near_send,
    near_recv,
    scatter_send,
    scatter_recv,
):
    me = lax.axis_index("fs")
    column = lax.axis_index("tp")
    n_a = 2 if n_fs % 2 == 0 else 1
    n_b = 2 if n_fs % 4 == 0 else 1
    plane = n_a * n_b
    n_z = n_fs // plane
    here_a = lax.rem(me, n_a)
    here_b = lax.rem(me // n_a, n_b)
    here_z = me // plane
    owns = (value_own, output_own, None, None)
    alls = (value_all, output_all, value_sum, output_sum)

    def index_of(z, flip_a, flip_b):
        a = n_a - 1 - here_a if flip_a else here_a
        b = n_b - 1 - here_b if flip_b else here_b
        return z * plane + b * n_a + a

    targets = {
        UP: me + plane,
        DOWN: me - plane,
        ACROSS_A: index_of(here_z, True, False),
        ACROSS_B: index_of(here_z, False, True),
    }
    can = {UP: here_z < n_z - 1, DOWN: here_z > 0, ACROSS_A: n_a > 1, ACROSS_B: n_b > 1}

    def copy_of(way, source, group, own):
        array, low, high, _, _ = GROUPS[group]
        there = alls[array].at[source] if low is None else alls[array].at[source, low:high]
        return pltpu.make_async_remote_copy(
            src_ref=owns[array].at[low:high] if own and low is not None else there,
            dst_ref=there,
            send_sem=gather_send.at[way, source, group],
            recv_sem=gather_recv.at[source, group],
            device_id={"fs": targets[way]},
            device_id_type=MESH,
        )

    def guarded(condition, action):
        if isinstance(condition, bool):
            if condition:
                action()
        else:
            pl.when(condition)(action)

    sent = []

    def send(way, source, group, own=False, valid=True):
        def begin():
            copy_of(way, source, group, own).start()

        def finish():
            copy_of(way, source, group, own).wait_send()

        condition = can[way]
        if valid is not True:
            condition = jnp.logical_and(condition, valid) if condition is not True else valid
        guarded(condition, begin)
        sent.append((condition, finish))

    def take(way, source, group):
        copy_of(way, source, group, False).wait_recv()

    def flips(axis):
        return axis == ACROSS_A, axis == ACROSS_B

    z_groups = [g for g in range(len(GROUPS)) if GROUPS[g][3] and GROUPS[g][0] < 2]
    plane_groups = [g for g in range(len(GROUPS)) if not GROUPS[g][3]]
    total_groups = [g for g in range(len(GROUPS)) if GROUPS[g][0] >= 2]

    value_own[...] = value_master[...].astype(jnp.bfloat16)
    output_own[...] = output_master[...].astype(jnp.bfloat16)
    loads = [
        pltpu.make_async_copy(src, dst, load_sem.at[i])
        for i, (src, dst) in enumerate(
            (
                (mixer_hbm, mixer),
                (output_factor_hbm, output_factor),
                (normed_hbm, normed),
                (value_factor_hbm, value_factor),
                (value_cot_hbm, value_cot_ref),
                (output_cot_hbm, output_cot_ref),
                (value_moment_hbm, value_moment),
                (value_second_hbm, value_second),
                (output_moment_hbm, output_moment),
                (output_second_hbm, output_second),
            )
        )
    ]
    for copy in loads:
        copy.start()

    for group in z_groups + plane_groups:
        for way in (UP, DOWN, ACROSS_A, ACROSS_B):
            send(way, me, group, own=True)
    keep = [
        pltpu.make_async_copy(owns[i], alls[i].at[me], local_sem.at[i]) for i in range(2)
    ]
    for copy in keep:
        copy.start()

    near = []
    for i, (tokens, factor, own, dst) in enumerate(
        (
            (mixer, output_factor, mixer_ref, near_mix),
            (normed, value_factor, input_ref, near_in),
        )
    ):
        loads[2 * i].wait()
        loads[2 * i + 1].wait()
        depth = tokens.shape[1]
        mine = factor[pl.ds(pl.multiple_of(column * depth, depth), depth), :]
        own[...] = jnp.dot(
            tokens[...], mine, preferred_element_type=jnp.float32
        ).astype(jnp.bfloat16)
        for k in range(1, n_tp):
            copy = pltpu.make_async_remote_copy(
                src_ref=own,
                dst_ref=dst.at[k - 1],
                send_sem=near_send.at[k - 1, i],
                recv_sem=near_recv.at[k - 1, i],
                device_id={"tp": lax.rem(column + k, n_tp)},
                device_id_type=MESH,
            )
            copy.start()
            near.append(copy)
    for copy in near:
        copy.wait()
    input_total = input_ref[...].astype(jnp.float32)
    mixer_total = mixer_ref[...].astype(jnp.float32)
    for k in range(n_tp - 1):
        input_total += near_in[k].astype(jnp.float32)
        mixer_total += near_mix[k].astype(jnp.float32)
    for copy in loads[4:]:
        copy.wait()
    across = (((0,), (0,)), ((), ()))
    rows = value_part.shape[1]
    scatter = []
    for i, (left, right, part, recv) in enumerate(
        (
            (input_total.astype(jnp.bfloat16), value_cot_ref, value_part, value_recv),
            (mixer_total.astype(jnp.bfloat16), output_cot_ref, output_part, output_recv),
        )
    ):
        width = right.shape[1]
        tile = 512 if width % 512 == 0 else width
        for c in range(width // tile):
            cols = slice(c * tile, (c + 1) * tile)
            product = lax.dot_general(
                left, right[:, cols], across, preferred_element_type=jnp.float32
            )
            for s in range(n_fs):
                part[s, :, cols] = product[s * rows : (s + 1) * rows]
        for k in range(1, n_fs):
            there = lax.rem(me + k, n_fs)
            copy = pltpu.make_async_remote_copy(
                src_ref=part.at[there],
                dst_ref=recv.at[k],
                send_sem=scatter_send.at[i, k],
                recv_sem=scatter_recv.at[i, k],
                device_id={"fs": there},
                device_id_type=MESH,
            )
            copy.start()
            scatter.append(copy)

    def plane_round():
        for group in plane_groups:
            first, second = GROUPS[group][4]
            if can[first]:
                source = index_of(here_z, *flips(first))
                take(first, source, group)
                for way in (second, UP, DOWN):
                    send(way, source, group)
        for group in plane_groups:
            first, second = GROUPS[group][4]
            if can[second]:
                for both in (False, True):
                    if both and not can[first]:
                        continue
                    source = index_of(
                        here_z,
                        second == ACROSS_A or (both and first == ACROSS_A),
                        second == ACROSS_B or (both and first == ACROSS_B),
                    )
                    take(second, source, group)
                    for way in (UP, DOWN):
                        send(way, source, group)

    def z_round(d, z_groups, plane_groups):
        for sign, onward in ((-1, UP), (1, DOWN)):
            z = here_z + sign * d
            valid = z >= 0 if sign < 0 else z <= n_z - 1

            for group in z_groups:
                source = index_of(z, False, False)

                @pl.when(valid)
                def _(group=group, source=source):
                    take(DOWN if onward == UP else UP, source, group)

                send(onward, source, group, valid=valid)
                for way in GROUPS[group][4]:
                    send(way, source, group, valid=valid)
            for group in plane_groups:
                for flip_a in range(n_a):
                    for flip_b in range(n_b):
                        source = index_of(z, flip_a == 1, flip_b == 1)

                        @pl.when(valid)
                        def _(group=group, source=source):
                            take(DOWN if onward == UP else UP, source, group)

                        send(onward, source, group, valid=valid)

    def column_round(d, z_groups):
        for sign in (-1, 1):
            if d == 0 and sign == 1:
                continue
            z = here_z + sign * d
            valid = True if d == 0 else (z >= 0 if sign < 0 else z <= n_z - 1)
            for group in z_groups:
                first, second = GROUPS[group][4]
                if not can[first]:
                    continue
                source = index_of(z, *flips(first))
                guarded(valid, functools.partial(take, first, source, group))
                send(second, source, group, valid=valid)

    def share_totals():
        for copy in scatter:
            copy.wait_recv()
        for group, part, recv, out in zip(
            total_groups, (value_part, output_part), (value_recv, output_recv), alls[2:]
        ):
            total = part[me]
            for k in range(1, n_fs):
                total += recv[k]
            out[me] = total
            for way in (UP, DOWN, ACROSS_A, ACROSS_B):
                send(way, me, group, own=True)

    def last_hop(groups):
        for group in groups:
            first, second = GROUPS[group][4]
            if can[second]:
                for z in range(n_z):
                    for both in (False, True):
                        if both and not can[first]:
                            continue
                        source = index_of(
                            z,
                            second == ACROSS_A or (both and first == ACROSS_A),
                            second == ACROSS_B or (both and first == ACROSS_B),
                        )
                        take(second, source, group)

    plane_round()
    column_round(0, z_groups)
    for d in range(1, n_z):
        z_round(d, z_groups, plane_groups)
        if d == 1:
            share_totals()
        else:
            column_round(d - 2, total_groups)
            z_round(d - 1, total_groups, ())
        column_round(d, z_groups)
    if n_z == 1:
        share_totals()
        column_round(0, total_groups)
    else:
        column_round(n_z - 2, total_groups)
        z_round(n_z - 1, total_groups, ())
        column_round(n_z - 1, total_groups)
    last_hop(total_groups)

    counts = []
    for i, (first, second, total, high, low) in enumerate(
        (
            (value_moment, value_second, value_sum, value_high, value_low),
            (output_moment, output_second, output_sum, output_high, output_low),
        )
    ):
        width = total.shape[2]
        counts.append(n_fs * rows * width * n_tp)
        gathered = jnp.zeros((rows, 128), jnp.float32)
        for s in range(n_fs):
            norm = moments(first[s], second[s], total[s])[2]
            rounded = norm.astype(jnp.bfloat16)
            high[s] = rounded
            low[s] = (norm - rounded.astype(jnp.float32)).astype(jnp.bfloat16)
            square = norm * norm
            for c in range(width // 128):
                gathered += square[:, c * 128 : (c + 1) * 128]
        squares[i] = gathered
    peers = [
        pltpu.make_async_remote_copy(
            src_ref=squares,
            dst_ref=near_squares.at[k - 1],
            send_sem=near_send.at[k - 1, 2],
            recv_sem=near_recv.at[k - 1, 2],
            device_id={"tp": lax.rem(column + k, n_tp)},
            device_id_type=MESH,
        )
        for k in range(1, n_tp)
    ]
    for copy in peers:
        copy.start()
    for copy in peers:
        copy.wait()
    for i in range(2):
        total = squares[i]
        for k in range(n_tp - 1):
            total += near_squares[k, i]
        total = jnp.sum(jnp.sum(total, axis=1, keepdims=True), axis=0, keepdims=True)
        scales[i] = jnp.broadcast_to(lax.rsqrt(total / counts[i] + FLOOR), (8, 128))

    last_hop(z_groups)
    for copy in scatter:
        copy.wait_send()
    for condition, finish in sent:
        guarded(condition, finish)
    for copy in keep:
        copy.wait()


def transfers(
    n_fs,
    n_tp,
    normed_input,
    mixer_output,
    value_cot,
    output_cot,
    value_factor,
    output_factor,
    olds,
    value_master,
    output_master,
):
    f32, bf16 = jnp.float32, jnp.bfloat16
    rank = value_factor.shape[1]
    rows = rank // n_fs
    tokens, value_cols = value_cot.shape
    output_cols = output_cot.shape[1]
    vmem = pl.BlockSpec(memory_space=pltpu.VMEM)
    hbm = pl.BlockSpec(memory_space=pltpu.HBM)
    groups = len(GROUPS)
    others = max(n_tp - 1, 1)
    dma = pltpu.SemaphoreType.DMA
    value_stack, output_stack = (n_fs, rows, value_cols), (n_fs, rows, output_cols)
    streamed = (
        normed_input, mixer_output, value_cot, output_cot, value_factor, output_factor, *olds
    )
    return pl.pallas_call(
        functools.partial(transfer_kernel, n_fs, n_tp),
        out_shape=(
            jax.ShapeDtypeStruct((n_fs,) + value_master.shape, bf16),
            jax.ShapeDtypeStruct((n_fs,) + output_master.shape, bf16),
            jax.ShapeDtypeStruct(value_stack, f32),
            jax.ShapeDtypeStruct(output_stack, f32),
            jax.ShapeDtypeStruct(value_stack, bf16),
            jax.ShapeDtypeStruct(value_stack, bf16),
            jax.ShapeDtypeStruct(output_stack, bf16),
            jax.ShapeDtypeStruct(output_stack, bf16),
            jax.ShapeDtypeStruct((2, 8, 128), f32),
        ),
        in_specs=[hbm] * len(streamed) + [vmem] * 2,
        out_specs=(hbm, hbm) + (vmem,) * 7,
        scratch_shapes=[pltpu.VMEM(x.shape, x.dtype) for x in streamed]
        + [
            dma((len(streamed),)),
            pltpu.VMEM(value_master.shape, bf16),
            pltpu.VMEM(output_master.shape, bf16),
            pltpu.VMEM((tokens, rank), bf16),
            pltpu.VMEM((tokens, rank), bf16),
            pltpu.VMEM((others, tokens, rank), bf16),
            pltpu.VMEM((others, tokens, rank), bf16),
            pltpu.VMEM((2, rows, 128), f32),
            pltpu.VMEM((others, 2, rows, 128), f32),
            pltpu.VMEM(value_stack, f32),
            pltpu.VMEM(output_stack, f32),
            pltpu.VMEM(value_stack, f32),
            pltpu.VMEM(output_stack, f32),
            dma((4, n_fs, groups)),
            dma((n_fs, groups)),
            dma((2,)),
            dma((others, 3)),
            dma((others, 3)),
            dma((2, n_fs)),
            dma((2, n_fs)),
        ],
        compiler_params=pltpu.CompilerParams(has_side_effects=True),
    )(*streamed, value_master, output_master)


def moments(first, second, projected):
    first_new = BETA_ONE * first + (1.0 - BETA_ONE) * projected
    second_new = BETA_TWO * second + (1.0 - BETA_TWO) * projected * projected
    normalized = first_new / (jnp.sqrt(second_new) + EPSILON)
    return (first_new, second_new, normalized)


def per_device(
    n_fs,
    n_tp,
    normed_input,
    value_cotangent,
    mixer_output,
    output_cotangent,
    value_factor,
    output_factor,
    value_master,
    value_moment,
    value_second,
    output_master,
    output_moment,
    output_second,
):
    row_index = lax.axis_index("fs")
    rank = value_factor.shape[1]

    def stacked(x):
        return x.reshape(n_fs, rank // n_fs, x.shape[1])

    def pieces(x):
        return x.reshape(PIECES, x.shape[0] // PIECES, x.shape[1])

    olds = [stacked(x) for x in (value_moment, value_second, output_moment, output_second)]
    (
        value_all,
        output_all,
        value_sum,
        output_sum,
        value_high,
        value_low,
        output_high,
        output_low,
        scales,
    ) = transfers(
        n_fs,
        n_tp,
        normed_input,
        mixer_output,
        value_cotangent,
        output_cotangent,
        value_factor,
        output_factor,
        olds,
        pieces(value_master),
        pieces(output_master),
    )
    value_moment_new, value_second_new, _ = moments(
        value_moment, value_second, value_sum.reshape(value_moment.shape)
    )
    output_moment_new, output_second_new, _ = moments(
        output_moment, output_second, output_sum.reshape(output_moment.shape)
    )

    def update(factor, high, low, scale, master, gathered):
        rows, cols = master.shape
        high, low = high.reshape(rank, cols), low.reshape(rank, cols)
        pair = jnp.concatenate([high, low], axis=0)
        double = jnp.concatenate([factor, factor], axis=1)
        here = lax.dynamic_slice_in_dim(double, row_index * rows, rows, 0)
        step = scale * jnp.dot(here, pair, preferred_element_type=jnp.float32)
        new = master - STEP_RATE * step
        full = jnp.dot(double, pair, preferred_element_type=jnp.float32)
        flat = gathered.reshape(n_fs * rows, cols).astype(jnp.float32)
        copy = (flat - (STEP_RATE * scale) * full).astype(jnp.bfloat16)
        return step, new, copy

    value_step, value_new, value_copy = update(
        value_factor, value_high, value_low, scales[0, 0, 0], value_master, value_all
    )
    output_step, output_new, output_copy = update(
        output_factor, output_high, output_low, scales[1, 0, 0], output_master, output_all
    )
    return (
        value_step,
        value_new,
        value_copy,
        value_moment_new,
        value_second_new,
        output_step,
        output_new,
        output_copy,
        output_moment_new,
        output_second_new,
    )


def solution(mesh):
    return jax.shard_map(
        functools.partial(per_device, mesh.shape["fs"], mesh.shape["tp"]),
        mesh=mesh,
        in_specs=(
            P("fs", "tp"),
            P("fs", "tp"),
            P("fs", "tp"),
            P("fs", "tp"),
            P(),
            P(),
            P("fs", "tp"),
            P(None, "tp"),
            P(None, "tp"),
            P("fs", "tp"),
            P(None, "tp"),
            P(None, "tp"),
        ),
        out_specs=(
            P("fs", "tp"),
            P("fs", "tp"),
            P(None, "tp"),
            P(None, "tp"),
            P(None, "tp"),
            P("fs", "tp"),
            P("fs", "tp"),
            P(None, "tp"),
            P(None, "tp"),
            P(None, "tp"),
        ),
        check_vma=False,
    )
```

profile of v0, /device:TPU:0, one launch (start us, length us, event | category | flops | bytes accessed | tf_op | source)
XLA Modules:
  0.0 211.6 jit_solution(1642659344058194610)
XLA Ops:
  0.6 0.0 copy-start
  0.7 2.0 constant_dynamic-update-slice_fusion.3
  2.6 1.9 constant_dynamic-update-slice_fusion.2
  4.5 0.0 copy-done
  4.5 0.2 constant_dynamic-update-slice_fusion.1
  4.7 0.2 constant_dynamic-update-slice_fusion
  4.9 180.2 %shard_map.195 = (bf16[16,8,32,1024]{3,2,1,0:T(8,128)(2,1)}, bf16[16,8,16,2048]{3,2,1,0:T(8,128)(2,1)}, f32[16,8,1024]{2,1,0:T(8,128)}, f32[16,8,2048]{2,1,0:T(8...) custom-call(bf16[512,2048]{1,0:T(8,128)(2,1)} %normed_hbm.1, ...), custom_call_target="tpu_custom_call" | custom-call | tf_op jit(solution)/shard_map/pallas_call | solution.py:438
  185.1 1.2 fusion.14
  187.6 0.0 copy-start.1
  187.6 0.0 copy-start.9
  187.7 0.0 copy-start.10
  187.7 0.0 copy-start.13
  187.7 9.9 %fusion = bf16[2048,2048]{1,0:T(8,128)(2,1)} fusion(bf16[2048,2048]{1,0:T(8,128)(2,1)} %bitcast.43, bf16[2048,256]{1,0:T(8,128)(2,1)} %constant_dynamic-update-slice_fusion.2, f32[]{:T(128)S(6)} %mul.124, bf16[128,2048]{1,0:T(8,128)(2,1)} %bitcast.36, bf16[128,2048]{1,0:T(8,128)(2,1)} %bitcast.34), kind=kOutput, calls=%fused_computation.1 | convolution fusion | flops 2166358016 | bytes 18874372 | tf_op jit(solution)/shard_map/dot_general | solution.py:551
  197.6 0.0 copy-done.1
  197.6 3.2 %multiply_subtract_fusion = (f32[128,2048]{1,0:T(8,128)}, f32[128,2048]{1,0:T(8,128)}) fusion(f32[128,2048]{1,0:T(8,128)S(1)} %copy-done.1, bf16[128,2048]{1,0:T(8,128)(2,1)S(1)} %bitcast.37, bf16[128,2048]{1,0:T(8,128)(2,1)S(1)} %bitcast.35, bf16[2048,256]{1,0:T(8,128)(2,1)} %constant_dynamic-update-slice_fusion.2, s32[]{:T(128)S(6)} %select_n.7, f32[]{:T(128)} %bitcast.11), kind=kOutput, calls=%fused_computation.11 | convolution fusion | flops 137101312 | bytes 4260356 | tf_op jit(solution)/shard_map/dot_general | solution.py:549
  200.8 0.0 copy-done.11
  200.8 0.0 copy-start.4
  200.8 4.7 %fusion.1 = bf16[4096,1024]{1,0:T(8,128)(2,1)} fusion(bf16[4096,1024]{1,0:T(8,128)(2,1)S(1)} %bitcast.42, bf16[4096,256]{1,0:T(8,128)(2,1)S(1)} %constant_dynamic-update-slice_fusion, f32[]{:T(128)S(6)} %mul.107, bf16[128,1024]{1,0:T(8,128)(2,1)S(1)} %bitcast.40, bf16[128,1024]{1,0:T(8,128)(2,1)S(1)} %bitcast.38), kind=kOutput, calls=%fused_computation.3 | convolution fusion | flops 2165309440 | bytes 19398660 | tf_op jit(solution)/shard_map/dot_general | solution.py:551
  205.5 0.0 copy-done.4
  205.6 2.4 %multiply_subtract_fusion.1 = (f32[256,1024]{1,0:T(8,128)}, f32[256,1024]{1,0:T(8,128)}) fusion(f32[256,1024]{1,0:T(8,128)S(1)} %copy-done.4, bf16[128,1024]{1,0:T(8,128)(2,1)S(1)} %bitcast.41, bf16[128,1024]{1,0:T(8,128)(2,1)S(1)} %bitcast.39, bf16[4096,256]{1,0:T(8,128)(2,1)S(1)} %constant_dynamic-update-slice_fusion, s32[]{:T(128)S(6)} %select_n.6, ...), kind=kOutput, calls=%fused_computation.12 | convolution fusion | flops 136052736 | bytes 3801096 | tf_op jit(solution)/shard_map/dot_general | solution.py:549
  208.0 1.1 fusion.4
  209.2 0.3 copy-done.2
  209.5 0.4 copy-done.3
  209.9 1.7 fusion.2
  (16 shorter events, 0.0 us)
Async XLA Ops:
  0.6 3.8 %copy-start = (bf16[4096,128]{1,0:T(8,128)(2,1)S(1)}, bf16[4096,128]{1,0:T(8,128)(2,1)}, u32[]{:S(2)}) copy-start(bf16[4096,128]{1,0:T(8,128)(2,1)} %value_factor_hbm.1) | copy-start | bytes 3145732
  187.6 10.0 %copy-start.1 = (f32[128,2048]{1,0:T(8,128)S(1)}, f32[128,2048]{1,0:T(8,128)}, u32[]{:S(2)}) copy-start(f32[128,2048]{1,0:T(8,128)} %param.21) | copy-start | bytes 3145732
  187.6 9.9 %copy-start.9 = (bf16[16,8,2048]{2,1,0:T(8,128)(2,1)S(1)}, bf16[16,8,2048]{2,1,0:T(8,128)(2,1)}, u32[]{:S(2)}) copy-start(bf16[16,8,2048]{2,1,0:T(8,128)(2,1)} %get-tuple-element.24) | copy-start | bytes 1572868
  187.7 9.9 %copy-start.10 = (bf16[16,8,2048]{2,1,0:T(8,128)(2,1)S(1)}, bf16[16,8,2048]{2,1,0:T(8,128)(2,1)}, u32[]{:S(2)}) copy-start(bf16[16,8,2048]{2,1,0:T(8,128)(2,1)} %get-tuple-element.25) | copy-start | bytes 1572868
  187.7 13.1 %copy-start.13 = (bf16[16,8,32,1024]{3,2,1,0:T(8,128)(2,1)S(1)}, bf16[16,8,32,1024]{3,2,1,0:T(8,128)(2,1)}, u32[]{:S(2)}) copy-start(bf16[16,8,32,1024]{3,2,1,0:T(8,128)(2,1)} %get-tuple-element.22) | copy-start | bytes 25165828
  197.6 3.2 %copy-start.11 = (bf16[16,8,1024]{2,1,0:T(8,128)(2,1)S(1)}, bf16[16,8,1024]{2,1,0:T(8,128)(2,1)}, u32[]{:S(2)}) copy-start(bf16[16,8,1024]{2,1,0:T(8,128)(2,1)} %get-tuple-element.20) | copy-start | bytes 786436
  197.6 3.2 %copy-start.12 = (bf16[16,8,1024]{2,1,0:T(8,128)(2,1)S(1)}, bf16[16,8,1024]{2,1,0:T(8,128)(2,1)}, u32[]{:S(2)}) copy-start(bf16[16,8,1024]{2,1,0:T(8,128)(2,1)} %get-tuple-element.21) | copy-start | bytes 786436
  200.8 4.7 %copy-start.4 = (f32[256,1024]{1,0:T(8,128)S(1)}, f32[256,1024]{1,0:T(8,128)}, u32[]{:S(2)}) copy-start(f32[256,1024]{1,0:T(8,128)} %param.18) | copy-start | bytes 3145732
  205.5 2.4 %copy-start.5 = (f32[128,1024]{1,0:T(8,128)S(1)}, f32[128,1024]{1,0:T(8,128)}, u32[]{:S(2)}) copy-start(f32[128,1024]{1,0:T(8,128)} %param.19) | copy-start | bytes 1572868
  205.5 2.4 %copy-start.6 = (f32[128,1024]{1,0:T(8,128)S(1)}, f32[128,1024]{1,0:T(8,128)}, u32[]{:S(2)}) copy-start(f32[128,1024]{1,0:T(8,128)} %param.20) | copy-start | bytes 1572868
  205.5 2.5 %copy-start.8 = (f32[16,8,1024]{2,1,0:T(8,128)S(1)}, f32[16,8,1024]{2,1,0:T(8,128)}, u32[]{:S(2)}) copy-start(f32[16,8,1024]{2,1,0:T(8,128)} %get-tuple-element.23) | copy-start | bytes 1572868
  205.6 3.6 %copy-start.7 = (f32[16,8,2048]{2,1,0:T(8,128)S(1)}, f32[16,8,2048]{2,1,0:T(8,128)}, u32[]{:S(2)}) copy-start(f32[16,8,2048]{2,1,0:T(8,128)} %get-tuple-element.27) | copy-start | bytes 3145732
  208.0 1.5 copy-start.2
  208.0 1.9 copy-start.3
where the time goes:
time: 212 us
  Pallas kernels  180 us (85%)
  matrix products  20.2 us (10%)
  local copies, waits for them, and re-layouts  6.27 us (3%)
  other arithmetic  2.8 us (1%)
    pallas_call x1, Pallas kernels, transfers(): pl.pallas_call(functools.partial(transfer_kernel, n_fs, n_tp), out_shape=...  180 us
    dot_general x2, matrix products, update(): full = jnp.dot(double, pair, preferred_element_type=jnp.float32)  14.6 us
    dot_general x2, matrix products, update(): step = scale * jnp.dot(here, pair, preferred_element_type=jnp.float32)  5.6 us

commit v1 on v0

v1 whole, which is shorter than its diff:
```python
import collections
import functools

import jax
import jax.numpy as jnp
from jax import lax
from jax.experimental import pallas as pl
from jax.experimental.pallas import tpu as pltpu
from jax.sharding import PartitionSpec as P

BETA_ONE = 0.8
BETA_TWO = 0.9
EPSILON = 1e-08
STEP_RATE = 0.005
FLOOR = 0.25

MESH = pl.DeviceIdType.MESH
A, B, UP, DOWN = range(4)
PLANE = 4
LATENCY = 3
LEAD = 1.25
FLIGHT = 1.75


def pieces_of(rows, cols):
    count = max(1, min(4, rows * cols * 2 // 131072))
    while rows % (16 * count):
        count -= 1
    return count


def classes_of(counts):
    out = []
    for array, count in enumerate(counts):
        for p in range(count):
            plane_first = count == 4 and p == 3
            out.append((array, p, plane_first, A if (p + array) % 2 == 0 else B))
    return out


def onward(n_z, classes, z, item, via):
    _, fa, fb, p = item
    _, _, plane_first, order = classes[p]
    up = [UP] if z < n_z - 1 else []
    down = [DOWN] if z > 0 else []
    if via is None:
        return [A, B] + up + down
    if via in (UP, DOWN):
        return (up if via == UP else down) + ([] if plane_first else [A, B])
    links = []
    if (fa, fb) == (1, 0) and order == A:
        links.append(B)
    if (fa, fb) == (0, 1) and order == B:
        links.append(A)
    return links + (up + down if plane_first else [])


def hops_left(n_z, classes, z, item, link):
    _, fa, fb, p = item
    _, _, plane_first, order = classes[p]
    if link in (UP, DOWN):
        return (n_z - 2 - z if link == UP else z - 1) + (0 if plane_first else 2)
    turn = 1 if link == order and (fa, fb) == (0, 0) else 0
    return turn + (max(n_z - 1 - z, z) if plane_first else 0)


def plan(n_z, classes, reserved):
    pool = collections.defaultdict(list)
    arriving = collections.defaultdict(list)
    sends = {z: [] for z in range(n_z)}
    takes = {z: [] for z in range(n_z)}
    busy = collections.defaultdict(int)
    for z in range(n_z):
        for p in range(len(classes)):
            item = (z, 0, 0, p)
            for link in onward(n_z, classes, z, item, None):
                pool[z, link].append((0, item))
    missing = n_z * (n_z * PLANE - 1) * len(classes)
    tick = 0
    while missing:
        for z, item, via in arriving.pop(tick, ()):
            for link in onward(n_z, classes, z, item, via):
                pool[z, link].append((tick, item))
        for z in range(n_z):
            toward = 1 if 2 * z < n_z else -1
            for link in range(4):
                held = [n for start, way, n in reserved if way == link and start == tick]
                if held:
                    busy[z, link] = tick + held[0]
                waiting = pool[z, link]
                if busy[z, link] > tick or not waiting:
                    continue
                best = max(
                    waiting,
                    key=lambda x: (
                        hops_left(n_z, classes, z, x[1], link),
                        -abs(x[1][0] - z),
                        (x[1][0] - z) * toward,
                        -x[1][3],
                        -x[0],
                        -x[1][1],
                        -x[1][2],
                    ),
                )
                waiting.remove(best)
                item = best[1]
                source, fa, fb, p = item
                sends[z].append((tick, link, item))
                if link == A:
                    there, got = z, (source, 1 - fa, fb, p)
                elif link == B:
                    there, got = z, (source, fa, 1 - fb, p)
                else:
                    there, got = z + (1 if link == UP else -1), item
                takes[there].append((tick, link, got))
                arriving[tick + LATENCY].append((there, got, link))
                busy[z, link] = tick + 1
                missing -= 1
        tick += 1
    return sends, takes


def mirrored(n_z, events):
    swap = {A: A, B: B, UP: DOWN, DOWN: UP}
    return sorted(
        (tick, swap[link], (n_z - 1 - s, fa, fb, p)) for tick, link, (s, fa, fb, p) in events
    )


def roles_of(n_z, sends, takes):
    pairs = n_z % 2 == 0 and all(
        sorted(x[z]) == mirrored(n_z, x[n_z - 1 - z])
        for x in (sends, takes)
        for z in range(n_z // 2)
    )
    roles = []
    for z in range(n_z // 2 if pairs else n_z):
        events = []
        done = {}
        for tick, link, (source, fa, fb, p) in sorted(takes[z]):
            item = (source - z, fa, fb, p)
            done[item] = tick + FLIGHT
            events.append((tick + FLIGHT, 0, "take", link, item))
        last = collections.defaultdict(float)
        for tick, link, (source, fa, fb, p) in sorted(sends[z]):
            item = (source - z, fa, fb, p)
            when = max(tick - LEAD, done.get(item, 0.0), last[link])
            if item not in done and tick <= 4:
                when = 0.0
            last[link] = when
            events.append((when, 1, "send", link, item))
            events.append((max(tick + 3.0, when + 2.0), 2, "sent", link, item))
        roles.append((sorted(events, key=lambda e: e[:2]), done))
    return pairs, roles


def levels_of(n_z, z):
    out = [0]
    for d in range(1, n_z):
        for offset in (d, -d):
            if 0 <= z + offset < n_z:
                out.append(offset)
    return out


def step_kernel(
    n_fs,
    n_tp,
    normed_hbm,
    mixer_hbm,
    value_cot_hbm,
    output_cot_hbm,
    value_factor_hbm,
    output_factor_hbm,
    value_moment_hbm,
    value_second_hbm,
    output_moment_hbm,
    output_second_hbm,
    value_master_hbm,
    output_master_hbm,
    value_step,
    value_new,
    value_copy,
    value_moment_new,
    value_second_new,
    output_step,
    output_new,
    output_copy,
    output_moment_new,
    output_second_new,
    normed,
    mixer,
    value_cot,
    output_cot,
    value_factor,
    output_factor,
    value_moment,
    value_second,
    output_moment,
    output_second,
    value_master,
    output_master,
    load_sem,
    value_all,
    output_all,
    input_ref,
    mixer_ref,
    near_in,
    near_mix,
    squares,
    near_squares,
    total,
    part,
    a_recv,
    b_part,
    b_recv,
    quarter,
    z_part,
    z_recv,
    shares,
    wide,
    high,
    low,
    near_send,
    near_recv,
    sum_send,
    sum_recv,
    share_send,
    share_recv,
    gather_send,
    gather_recv,
):
    f32, bf16 = jnp.float32, jnp.bfloat16
    me = lax.axis_index("fs")
    column = lax.axis_index("tp")
    n_z = n_fs // PLANE
    half = n_fs // 2
    here_a = lax.rem(me, 2)
    here_b = lax.rem(me // 2, 2)
    here_z = me // PLANE
    alls = (value_all, output_all)
    rows = total.shape[1]
    cols = (value_cot.shape[1], output_cot.shape[1])
    starts = (0, cols[0])
    classes = classes_of([x.shape[1] for x in alls])
    fine = len(classes) == 8

    if fine:
        reserved = (
            (4, A, 3),
            (9, B, 2),
            (13, UP, 2),
            (13, DOWN, 2),
            (17, UP, 2),
            (17, DOWN, 2),
            (21, A, 2),
            (25, B, 3),
        )
        stages = (7.8, 11.8, 15.8, 19.8, 23.8, 28.8)
    else:
        reserved = ()
        stages = tuple(7.8 + 4 * i for i in range(6))
    sends, takes = plan(n_z, classes, reserved)
    pairs, roles = roles_of(n_z, sends, takes)
    if pairs:
        toward = jnp.where(2 * here_z < n_z, 1, -1)
        role = jnp.where(2 * here_z < n_z, here_z, n_z - 1 - here_z)
    else:
        toward = 1
        role = here_z

    across_a = me + 1 - 2 * here_a
    across_b = me + 2 - 4 * here_b
    targets = {
        A: across_a,
        B: across_b,
        UP: me + toward * PLANE,
        DOWN: me - toward * PLANE,
    }
    places = {
        (fa, fb): (1 - here_b if fb else here_b) * 2 + (1 - here_a if fa else here_a)
        for fa in range(2)
        for fb in range(2)
    }

    def z_mate(k):
        return lax.rem(here_z + k, n_z) * PLANE + lax.rem(me, PLANE)

    barrier = pltpu.get_barrier_semaphore()
    for there in [across_a, across_b] + [z_mate(k) for k in range(1, n_z)]:
        pl.semaphore_signal(barrier, inc=1, device_id={"fs": there}, device_id_type=MESH)
    for k in range(1, n_tp):
        pl.semaphore_signal(
            barrier,
            inc=1,
            device_id={"tp": lax.rem(column + k, n_tp)},
            device_id_type=MESH,
        )

    loads = [
        pltpu.make_async_copy(src, dst, load_sem.at[i])
        for i, (src, dst) in enumerate(
            (
                (value_master_hbm, value_master),
                (output_master_hbm, output_master),
                (mixer_hbm, mixer),
                (output_factor_hbm, output_factor),
                (normed_hbm, normed),
                (value_factor_hbm, value_factor),
                (value_cot_hbm, value_cot),
                (output_cot_hbm, output_cot),
                (value_moment_hbm, value_moment),
                (value_second_hbm, value_second),
                (output_moment_hbm, output_moment),
                (output_second_hbm, output_second),
            )
        )
    ]
    for copy in loads:
        copy.start()
    for i, master in enumerate((value_master, output_master)):
        loads[i].wait()
        height = alls[i].shape[2]
        for p in range(alls[i].shape[1]):
            alls[i][me, p] = master[p * height : (p + 1) * height, :].astype(bf16)
    pl.semaphore_wait(barrier, 2 + (n_z - 1) + (n_tp - 1))

    def piece_copy(link, item):
        offset, fa, fb, p = item
        source = (here_z + toward * offset) * PLANE + places[fa, fb]
        array, piece, _, _ = classes[p]
        there = alls[array].at[source, piece]
        return pltpu.make_async_remote_copy(
            src_ref=there,
            dst_ref=there,
            send_sem=gather_send.at[link, source, p],
            recv_sem=gather_recv.at[source, p],
            device_id={"fs": targets[link]},
            device_id_type=MESH,
        )

    def run_events(k, first, last):
        events = [e for e in roles[k][0] if first <= e[0] < last]
        if not events:
            return

        @pl.when(role == k)
        def _():
            for _, _, kind, link, item in events:
                copy = piece_copy(link, item)
                if kind == "take":
                    copy.wait_recv()
                elif kind == "send":
                    copy.start()
                else:
                    copy.wait_send()

    def message(src, dst, there, sems, index):
        send, recv = sems
        return pltpu.make_async_remote_copy(
            src_ref=src,
            dst_ref=dst,
            send_sem=send.at[index],
            recv_sem=recv.at[index],
            device_id={"fs": there},
            device_id_type=MESH,
        )

    sums = (sum_send, sum_recv)
    shared = (share_send, share_recv)
    pending = []

    def start(copies):
        for copy in copies:
            copy.start()
        pending.extend(copies)
        return copies

    a_sum = message(part.at[pl.ds((1 - here_a) * half, half)], a_recv, across_a, sums, 0)
    b_sum = message(b_part, b_recv, across_b, sums, n_z)
    z_sums = [
        message(z_part.at[lax.rem(here_z + k, n_z)], z_recv.at[k], z_mate(k), sums, k)
        for k in range(1, n_z)
    ]
    mine = here_a * half + here_b * n_z
    z_shares = [
        message(shares.at[mine + here_z], shares.at[mine + here_z], z_mate(k), shared, k)
        for k in range(1, n_z)
    ]
    ours = shares.at[pl.ds(mine, n_z)]
    other = shares.at[pl.ds((1 - here_a) * half + here_b * n_z, n_z)]
    a_share = message(ours, ours, across_a, shared, 0)
    b_shares = [
        message(ours, ours, across_b, shared, n_z),
        message(other, other, across_b, shared, n_z + 1),
    ]

    def products():
        near = []
        for i, (tokens, factor, own, dst) in enumerate(
            (
                (mixer, output_factor, mixer_ref, near_mix),
                (normed, value_factor, input_ref, near_in),
            )
        ):
            loads[2 + 2 * i].wait()
            loads[3 + 2 * i].wait()
            depth = tokens.shape[1]
            rows_here = factor[pl.ds(pl.multiple_of(column * depth, depth), depth), :]
            own[...] = jnp.dot(
                tokens[...], rows_here, preferred_element_type=f32
            ).astype(bf16)
            for k in range(1, n_tp):
                copy = pltpu.make_async_remote_copy(
                    src_ref=own,
                    dst_ref=dst.at[k - 1],
                    send_sem=near_send.at[k - 1, i],
                    recv_sem=near_recv.at[k - 1, i],
                    device_id={"tp": lax.rem(column + k, n_tp)},
                    device_id_type=MESH,
                )
                copy.start()
                near.append(copy)
        for copy in near:
            copy.wait()
        input_total = input_ref[...].astype(f32)
        mixer_total = mixer_ref[...].astype(f32)
        for k in range(n_tp - 1):
            input_total += near_in[k].astype(f32)
            mixer_total += near_mix[k].astype(f32)
        for copy in loads[6:8]:
            copy.wait()
        across = (((0,), (0,)), ((), ()))
        for i, (left, right) in enumerate(
            (
                (input_total.astype(bf16), value_cot),
                (mixer_total.astype(bf16), output_cot),
            )
        ):
            tile = 512 if cols[i] % 512 == 0 else cols[i]
            for c in range(cols[i] // tile):
                product = lax.dot_general(
                    left,
                    right[:, c * tile : (c + 1) * tile],
                    across,
                    preferred_element_type=f32,
                )
                at = slice(starts[i] + c * tile, starts[i] + (c + 1) * tile)
                for s in range(n_fs):
                    block = product[s * rows : (s + 1) * rows]
                    total[s, :, at] = block
                    part[s, :, at] = block.astype(bf16)
        start([a_sum])

    def second_sum():
        a_sum.wait_recv()
        away = (1 - here_b) * n_z
        b_part[...] = (
            total[pl.ds(here_a * half + away, n_z)] + a_recv[pl.ds(away, n_z)].astype(f32)
        ).astype(bf16)
        start([b_sum])
        quarter[...] = total[pl.ds(mine, n_z)] + a_recv[pl.ds(here_b * n_z, n_z)].astype(f32)

    def third_sum():
        b_sum.wait_recv()
        quarter[...] += b_recv[...].astype(f32)
        z_part[...] = quarter[...].astype(bf16)
        start(z_sums)

    def last_sum():
        for copy in z_sums:
            copy.wait_recv()
        done = quarter[here_z]
        for k in range(1, n_z):
            done += z_recv[k].astype(f32)
        shares[mine + here_z] = done.astype(bf16)
        start(z_shares)

    def share_a():
        for copy in z_shares:
            copy.wait_recv()
        start([a_share])

    def share_b():
        a_share.wait_recv()
        start(b_shares)

    square_copies = [
        pltpu.make_async_remote_copy(
            src_ref=squares,
            dst_ref=near_squares.at[k - 1],
            send_sem=near_send.at[k - 1, 2],
            recv_sem=near_recv.at[k - 1, 2],
            device_id={"tp": lax.rem(column + k, n_tp)},
            device_id_type=MESH,
        )
        for k in range(1, n_tp)
    ]
    rank = value_factor.shape[1]
    block = 16

    def moments():
        for copy in b_shares:
            copy.wait_recv()
        for copy in loads[8:]:
            copy.wait()
        for s in range(n_fs):
            wide[s * rows : (s + 1) * rows, :] = shares[s].astype(f32)
        for i, (first, second, first_new, second_new) in enumerate(
            (
                (value_moment, value_second, value_moment_new, value_second_new),
                (output_moment, output_second, output_moment_new, output_second_new),
            )
        ):
            span = slice(starts[i], starts[i] + cols[i])

            def body(r, gathered, first=first, second=second, first_new=first_new,
                     second_new=second_new, span=span, i=i):
                at = pl.ds(pl.multiple_of(r * block, block), block)
                projected = wide[at, span]
                m = BETA_ONE * first[at, :] + (1.0 - BETA_ONE) * projected
                v = BETA_TWO * second[at, :] + (1.0 - BETA_TWO) * projected * projected
                norm = m / (jnp.sqrt(v) + EPSILON)
                first_new[at, :] = m
                second_new[at, :] = v
                wide[at, span] = norm
                square = norm * norm
                square = square[:8] + square[8:]
                for c in range(cols[i] // 128):
                    gathered += square[:, c * 128 : (c + 1) * 128]
                return gathered

            squares[i] = lax.fori_loop(
                0, rank // block, body, jnp.zeros((8, 128), f32)
            )
        for copy in square_copies:
            copy.start()

    def steps():
        for copy in square_copies:
            copy.wait()
        for i, (factor, master, step, new) in enumerate(
            (
                (value_factor, value_master, value_step, value_new),
                (output_factor, output_master, output_step, output_new),
            )
        ):
            gathered = squares[i]
            for k in range(n_tp - 1):
                gathered += near_squares[k, i]
            gathered = jnp.sum(jnp.sum(gathered, axis=1, keepdims=True), axis=0, keepdims=True)
            scale = lax.rsqrt(gathered / (rank * cols[i] * n_tp) + FLOOR)
            span = slice(starts[i], starts[i] + cols[i])

            def body(r, carry, span=span, scale=scale, width=cols[i]):
                at = pl.ds(pl.multiple_of(r * block, block), block)
                scaled = wide[at, span] * jnp.broadcast_to(scale, (block, width))
                rounded = scaled.astype(bf16)
                high[at, span] = rounded
                low[at, span] = (scaled - rounded.astype(f32)).astype(bf16)
                return carry

            lax.fori_loop(0, rank // block, body, 0)
            height = master.shape[0]
            here = factor[pl.ds(pl.multiple_of(me * height, height), height), :]
            tile = 512 if cols[i] % 512 == 0 else cols[i]
            for c in range(cols[i] // tile):
                at = slice(c * tile, (c + 1) * tile)
                inner = slice(starts[i] + c * tile, starts[i] + (c + 1) * tile)
                moved = jnp.dot(here, high[:, inner], preferred_element_type=f32) + jnp.dot(
                    here, low[:, inner], preferred_element_type=f32
                )
                step[:, at] = moved
                new[:, at] = master[:, at] - STEP_RATE * moved

    def copies(level, i, pieces):
        if pairs:
            offset = jnp.int32(0)
            for k in range(len(roles)):
                offset = jnp.where(role == k, levels_of(n_z, k)[level], offset)
            source_z = here_z + toward * offset
        else:
            offset = jnp.int32(0)
            for k in range(len(roles)):
                offset = jnp.where(role == k, levels_of(n_z, k)[level], offset)
            source_z = here_z + offset
        factor = (value_factor, output_factor)[i]
        out = (value_copy, output_copy)[i]
        height = alls[i].shape[2]
        tall = alls[i].shape[1] * height
        tile = 512 if cols[i] % 512 == 0 else cols[i]

        def body(c, carry):
            source = source_z * PLANE + c
            base = pl.multiple_of(source * tall, tall) + pieces[0] * height
            base = pl.multiple_of(base, height)
            here = factor[pl.ds(base, len(pieces) * height), :]
            for t in range(cols[i] // tile):
                at = slice(t * tile, (t + 1) * tile)
                inner = slice(starts[i] + t * tile, starts[i] + (t + 1) * tile)
                moved = jnp.dot(here, high[:, inner], preferred_element_type=f32)
                for n, p in enumerate(pieces):
                    old = alls[i][source, p, :, at].astype(f32)
                    fresh = old - STEP_RATE * moved[n * height : (n + 1) * height]
                    out[pl.ds(pl.multiple_of(base + n * height, height), height), at] = (
                        fresh.astype(bf16)
                    )
            return carry

        lax.fori_loop(0, PLANE, body, 0)

    work = [
        (0.5, products),
        (stages[0], second_sum),
        (stages[1], third_sum),
        (stages[2], last_sum),
        (stages[3], share_a),
        (stages[4], share_b),
        (stages[5], moments),
        (stages[5] + 0.5, steps),
    ]
    free = stages[5] + 0.6
    ready = []
    for level in range(n_z):
        for i in range(2):
            count = alls[i].shape[1]
            groups = [tuple(range(count))]
            if level == n_z - 1:
                groups = [(p,) for p in range(count)]
            for pieces in groups:
                when = 0.0
                for k in range(len(roles)):
                    offset = levels_of(n_z, k)[level]
                    for item, at in roles[k][1].items():
                        array, p, _, _ = classes[item[3]]
                        if item[0] == offset and array == i and p in pieces:
                            when = max(when, at)
                ready.append((when, len(ready), level, i, pieces))
    for when, _, level, i, pieces in sorted(ready):
        free = max(free + 0.45 * len(pieces) / alls[i].shape[1], when + 0.01)
        work.append((free, functools.partial(copies, level, i, pieces)))

    before = -1.0
    for when, action in sorted(work, key=lambda x: x[0]):
        for k in range(len(roles)):
            run_events(k, before, when)
        action()
        before = when
    for k in range(len(roles)):
        run_events(k, before, float("inf"))
    for copy in pending:
        copy.wait_send()


def per_device(
    n_fs,
    n_tp,
    normed_input,
    value_cotangent,
    mixer_output,
    output_cotangent,
    value_factor,
    output_factor,
    value_master,
    value_moment,
    value_second,
    output_master,
    output_moment,
    output_second,
):
    f32, bf16 = jnp.float32, jnp.bfloat16
    rank = value_factor.shape[1]
    rows = rank // n_fs
    n_z = n_fs // PLANE
    tokens, value_cols = value_cotangent.shape
    output_cols = output_cotangent.shape[1]
    both = value_cols + output_cols
    others = max(n_tp - 1, 1)
    dma = pltpu.SemaphoreType.DMA
    stacks = []
    for master in (value_master, output_master):
        count = pieces_of(*master.shape)
        stacks.append((n_fs, count, master.shape[0] // count, master.shape[1]))
    n_pieces = stacks[0][1] + stacks[1][1]
    streamed = (
        normed_input,
        mixer_output,
        value_cotangent,
        output_cotangent,
        value_factor,
        output_factor,
        value_moment,
        value_second,
        output_moment,
        output_second,
        value_master,
        output_master,
    )
    outs = []
    for master, moment in ((value_master, value_moment), (output_master, output_moment)):
        outs += [
            (master.shape, f32),
            (master.shape, f32),
            ((n_fs * master.shape[0], master.shape[1]), bf16),
            (moment.shape, f32),
            (moment.shape, f32),
        ]
    return pl.pallas_call(
        functools.partial(step_kernel, n_fs, n_tp),
        out_shape=tuple(pltpu.VMEM(*x) for x in outs),
        in_specs=[pl.BlockSpec(memory_space=pltpu.HBM)] * len(streamed),
        out_specs=(pl.BlockSpec(memory_space=pltpu.VMEM),) * len(outs),
        scratch_shapes=[pltpu.VMEM(x.shape, x.dtype) for x in streamed]
        + [
            dma((len(streamed),)),
            pltpu.VMEM(stacks[0], bf16),
            pltpu.VMEM(stacks[1], bf16),
            pltpu.VMEM((tokens, rank), bf16),
            pltpu.VMEM((tokens, rank), bf16),
            pltpu.VMEM((others, tokens, rank), bf16),
            pltpu.VMEM((others, tokens, rank), bf16),
            pltpu.VMEM((2, 8, 128), f32),
            pltpu.VMEM((others, 2, 8, 128), f32),
            pltpu.VMEM((n_fs, rows, both), f32),
            pltpu.VMEM((n_fs, rows, both), bf16),
            pltpu.VMEM((n_fs // 2, rows, both), bf16),
            pltpu.VMEM((n_z, rows, both), bf16),
            pltpu.VMEM((n_z, rows, both), bf16),
            pltpu.VMEM((n_z, rows, both), f32),
            pltpu.VMEM((n_z, rows, both), bf16),
            pltpu.VMEM((n_z, rows, both), bf16),
            pltpu.VMEM((n_fs, rows, both), bf16),
            pltpu.VMEM((rank, both), f32),
            pltpu.VMEM((rank, both), bf16),
            pltpu.VMEM((rank, both), bf16),
            dma((others, 3)),
            dma((others, 3)),
            dma((n_z + 1,)),
            dma((n_z + 1,)),
            dma((n_z + 2,)),
            dma((n_z + 2,)),
            dma((4, n_fs, n_pieces)),
            dma((n_fs, n_pieces)),
        ],
        compiler_params=pltpu.CompilerParams(
            collective_id=0, has_side_effects=True, vmem_limit_bytes=39 << 20
        ),
    )(*streamed)


def solution(mesh):
    return jax.shard_map(
        functools.partial(per_device, mesh.shape["fs"], mesh.shape["tp"]),
        mesh=mesh,
        in_specs=(
            P("fs", "tp"),
            P("fs", "tp"),
            P("fs", "tp"),
            P("fs", "tp"),
            P(),
            P(),
            P("fs", "tp"),
            P(None, "tp"),
            P(None, "tp"),
            P("fs", "tp"),
            P(None, "tp"),
            P(None, "tp"),
        ),
        out_specs=(
            P("fs", "tp"),
            P("fs", "tp"),
            P(None, "tp"),
            P(None, "tp"),
            P(None, "tp"),
            P("fs", "tp"),
            P("fs", "tp"),
            P(None, "tp"),
            P(None, "tp"),
            P(None, "tp"),
        ),
        check_vma=False,
    )
```

time: 212 us -> 159 us (0.75)
  Pallas kernels: 180 us -> 144 us
  matrix products: 20.2 us -> 0 us
  local copies, waits for them, and re-layouts: 6.27 us -> 14.2 us
  other arithmetic: 2.8 us -> 0 us
    pallas_call x1, Pallas kernels: 180 us -> 144 us  [per_device(): pl.pallas_call(functools.partial(step_kernel, n_fs, n_tp), out_shape=tupl...]
    dot_general x4 -> x0, matrix products: 20.2 us -> none  [the longest x2 14.6 us: update(): full = jnp.dot(double, pair, preferred_element_type=jnp.float32)]
    unnamed x30 -> x10, local copies, waits for them, and re-layouts: 2.95 us -> 14.2 us
    add x2 -> x0, other arithmetic: 2.8 us -> none  [moments(): second_new = BETA_TWO * second + (1.0 - BETA_TWO) * projected * projected]
where the time goes in v1:
time: 159 us
  Pallas kernels  144 us (91%)
  local copies, waits for them, and re-layouts  14.2 us (9%)
    pallas_call x1, Pallas kernels, per_device(): pl.pallas_call(functools.partial(step_kernel, n_fs, n_tp), out_shape=tupl...  144 us
    unnamed x10, local copies, waits for them, and re-layouts  14.2 us

profile of v1, /device:TPU:0, one launch (start us, length us, event | category | flops | bytes accessed | tf_op | source)
XLA Modules:
  0.0 159.2 jit_solution(13125811467202746031)
XLA Ops:
  0.6 144.4 %shard_map.195 = (f32[256,1024]{1,0:T(8,128)S(1)}, f32[256,1024]{1,0:T(8,128)S(1)}, bf16[4096,1024]{1,0:T(8,128)(2,1)S(1)}, f32[128,1024]{1,0:T(8,128)S(1)}, f32...) custom-call(bf16[512,2048]{1,0:T(8,128)(2,1)} %normed_hbm.1, ...), custom_call_target="tpu_custom_call" | custom-call | tf_op jit(solution)/shard_map/pallas_call | solution.py:708
  145.0 1.0 copy.32
  146.0 0.8 copy.35
  146.8 0.8 copy.36
  147.6 1.0 copy.33
  148.6 1.0 copy.37
  149.5 1.0 copy.38
  150.5 1.0 copy.40
  151.5 1.0 copy.41
  152.4 3.4 %copy.34 = bf16[4096,1024]{1,0:T(8,128)(2,1)} copy(bf16[4096,1024]{1,0:T(8,128)(2,1)S(1)} %get-tuple-element.12) | data formatting | bytes 16777216
  155.8 3.4 %copy.39 = bf16[2048,2048]{1,0:T(8,128)(2,1)} copy(bf16[2048,2048]{1,0:T(8,128)(2,1)S(1)} %get-tuple-element.17) | data formatting | bytes 16777216

commit v2 on v1

--- a/solution.py
+++ b/solution.py
@@ -1,5 +1,6 @@
 import collections
 import functools
+import math
 
 import jax
 import jax.numpy as jnp
@@ -17,13 +18,14 @@
 MESH = pl.DeviceIdType.MESH
 A, B, UP, DOWN = range(4)
 PLANE = 4
-LATENCY = 3
-LEAD = 1.25
+GRAIN = 1
+LATENCY = 6
+LEAD = 3.0
 FLIGHT = 1.75
 
 
 def pieces_of(rows, cols):
-    count = max(1, min(4, rows * cols * 2 // 131072))
+    count = max(1, min(4 * GRAIN, rows * cols * 2 * GRAIN // 131072))
     while rows % (16 * count):
         count -= 1
     return count
@@ -33,7 +35,7 @@
     out = []
     for array, count in enumerate(counts):
         for p in range(count):
-            plane_first = count == 4 and p == 3
+            plane_first = count % 4 == 0 and p % 4 == 3
             out.append((array, p, plane_first, A if (p + array) % 2 == 0 else B))
     return out
 
@@ -84,7 +86,11 @@
         for z in range(n_z):
             toward = 1 if 2 * z < n_z else -1
             for link in range(4):
-                held = [n for start, way, n in reserved if way == link and start == tick]
+                held = [
+                    n * GRAIN
+                    for start, way, n in reserved
+                    if way == link and start * GRAIN == tick
+                ]
                 if held:
                     busy[z, link] = tick + held[0]
                 waiting = pool[z, link]
@@ -113,7 +119,7 @@
                 else:
                     there, got = z + (1 if link == UP else -1), item
                 takes[there].append((tick, link, got))
-                arriving[tick + LATENCY].append((there, got, link))
+                arriving[tick + LATENCY * GRAIN].append((there, got, link))
                 busy[z, link] = tick + 1
                 missing -= 1
         tick += 1
@@ -139,28 +145,59 @@
         done = {}
         for tick, link, (source, fa, fb, p) in sorted(takes[z]):
             item = (source - z, fa, fb, p)
-            done[item] = tick + FLIGHT
-            events.append((tick + FLIGHT, 0, "take", link, item))
+            done[item] = tick / GRAIN + FLIGHT
+            events.append((done[item], 0, "take", link, item))
         last = collections.defaultdict(float)
         for tick, link, (source, fa, fb, p) in sorted(sends[z]):
             item = (source - z, fa, fb, p)
-            when = max(tick - LEAD, done.get(item, 0.0), last[link])
-            if item not in done and tick <= 4:
+            at = tick / GRAIN
+            when = max(at - LEAD, done.get(item, 0.0), last[link])
+            if item not in done and at <= 4:
                 when = 0.0
             last[link] = when
             events.append((when, 1, "send", link, item))
-            events.append((max(tick + 3.0, when + 2.0), 2, "sent", link, item))
+            events.append((max(at + 3.0, when + 2.0), 2, "sent", link, item))
         roles.append((sorted(events, key=lambda e: e[:2]), done))
     return pairs, roles
 
 
 def levels_of(n_z, z):
-    out = [0]
-    for d in range(1, n_z):
-        for offset in (d, -d):
-            if 0 <= z + offset < n_z:
-                out.append(offset)
+    near, toward = (z, 1) if 2 * z < n_z else (n_z - 1 - z, -1)
+    out = []
+    for level in range(n_z):
+        step = (level + 1) // 2 if level % 2 else -(level // 2)
+        out.append(toward * (step if level <= 2 * near else level - near))
     return out
+
+
+def level_z(n_z, here_z, level):
+    near = jnp.where(2 * here_z < n_z, here_z, n_z - 1 - here_z)
+    toward = jnp.where(2 * here_z < n_z, 1, -1)
+    step = (level + 1) // 2 if level % 2 else -(level // 2)
+    return here_z + toward * jnp.where(level <= 2 * near, step, level - near)
+
+
+def renew(source_z, factor, high, start, old, out, first):
+    _, count, height, cols = old.shape
+    tall = count * height
+    tile = 512 if cols % 512 == 0 else cols
+
+    def body(c, carry):
+        source = source_z * PLANE + c
+        here = factor[pl.ds(pl.multiple_of(source * tall, tall), tall), :]
+        for t in range(cols // tile):
+            at = slice(t * tile, (t + 1) * tile)
+            inner = slice(start + t * tile, start + (t + 1) * tile)
+            moved = jnp.dot(here, high[:, inner], preferred_element_type=jnp.float32)
+            for p in range(count):
+                fresh = (
+                    old[source, p, :, at].astype(jnp.float32)
+                    - STEP_RATE * moved[p * height : (p + 1) * height]
+                )
+                out[first + c, p, :, at] = fresh.astype(jnp.bfloat16)
+        return carry
+
+    lax.fori_loop(0, PLANE, body, 0)
 
 
 def step_kernel(
@@ -180,20 +217,21 @@
     output_master_hbm,
     value_step,
     value_new,
-    value_copy,
+    value_all,
     value_moment_new,
     value_second_new,
     output_step,
     output_new,
-    output_copy,
+    output_all,
     output_moment_new,
     output_second_new,
+    value_factor,
+    output_factor,
+    high,
     normed,
     mixer,
     value_cot,
     output_cot,
-    value_factor,
-    output_factor,
     value_moment,
     value_second,
     output_moment,
@@ -201,8 +239,7 @@
     value_master,
     output_master,
     load_sem,
-    value_all,
-    output_all,
+    master_sem,
     input_ref,
     mixer_ref,
     near_in,
@@ -219,7 +256,6 @@
     z_recv,
     shares,
     wide,
-    high,
     low,
     near_send,
     near_recv,
@@ -243,20 +279,20 @@
     cols = (value_cot.shape[1], output_cot.shape[1])
     starts = (0, cols[0])
     classes = classes_of([x.shape[1] for x in alls])
-    fine = len(classes) == 8
+    fine = len(classes) == 8 * GRAIN
 
     if fine:
         reserved = (
             (4, A, 3),
-            (9, B, 2),
-            (13, UP, 2),
-            (13, DOWN, 2),
-            (17, UP, 2),
-            (17, DOWN, 2),
-            (21, A, 2),
-            (25, B, 3),
+            (10, B, 2),
+            (15, UP, 1),
+            (15, DOWN, 1),
+            (20, UP, 1),
+            (20, DOWN, 1),
+            (25, A, 2),
+            (30, B, 3),
         )
-        stages = (7.8, 11.8, 15.8, 19.8, 23.8, 28.8)
+        stages = (7.8, 12.8, 17.8, 22.8, 27.8, 33.8)
     else:
         reserved = ()
         stages = tuple(7.8 + 4 * i for i in range(6))
@@ -286,23 +322,18 @@
     def z_mate(k):
         return lax.rem(here_z + k, n_z) * PLANE + lax.rem(me, PLANE)
 
-    barrier = pltpu.get_barrier_semaphore()
-    for there in [across_a, across_b] + [z_mate(k) for k in range(1, n_z)]:
-        pl.semaphore_signal(barrier, inc=1, device_id={"fs": there}, device_id_type=MESH)
-    for k in range(1, n_tp):
-        pl.semaphore_signal(
-            barrier,
-            inc=1,
-            device_id={"tp": lax.rem(column + k, n_tp)},
-            device_id_type=MESH,
+    masters = []
+    for array, p, _, _ in classes:
+        hbm, master = ((value_master_hbm, value_master), (output_master_hbm, output_master))[array]
+        height = alls[array].shape[2]
+        at = pl.ds(p * height, height)
+        masters.append(
+            pltpu.make_async_copy(hbm.at[at], master.at[at], master_sem.at[len(masters)])
         )
-
     loads = [
         pltpu.make_async_copy(src, dst, load_sem.at[i])
         for i, (src, dst) in enumerate(
             (
-                (value_master_hbm, value_master),
-                (output_master_hbm, output_master),
                 (mixer_hbm, mixer),
                 (output_factor_hbm, output_factor),
                 (normed_hbm, normed),
@@ -316,14 +347,31 @@
             )
         )
     ]
-    for copy in loads:
-        copy.start()
-    for i, master in enumerate((value_master, output_master)):
-        loads[i].wait()
-        height = alls[i].shape[2]
-        for p in range(alls[i].shape[1]):
-            alls[i][me, p] = master[p * height : (p + 1) * height, :].astype(bf16)
-    pl.semaphore_wait(barrier, 2 + (n_z - 1) + (n_tp - 1))
+
+    opening = [[] for _ in classes]
+    for k, (events, _) in enumerate(roles):
+        for when, _, kind, link, item in events:
+            if kind == "send" and when == 0.0:
+                opening[item[3]].append((k, link, item))
+    queue = sorted(
+        range(len(classes)),
+        key=lambda p: min(
+            [t for z in sends for t, _, item in sends[z] if item == (z, 0, 0, p)]
+        ),
+    )
+    for p in queue:
+        masters[p].start()
+
+    barrier = pltpu.get_barrier_semaphore()
+    for there in [across_a, across_b] + [z_mate(k) for k in range(1, n_z)]:
+        pl.semaphore_signal(barrier, inc=1, device_id={"fs": there}, device_id_type=MESH)
+    for k in range(1, n_tp):
+        pl.semaphore_signal(
+            barrier,
+            inc=1,
+            device_id={"tp": lax.rem(column + k, n_tp)},
+            device_id_type=MESH,
+        )
 
     def piece_copy(link, item):
         offset, fa, fb, p = item
@@ -339,8 +387,35 @@
             device_id_type=MESH,
         )
 
+    def open_piece(p):
+        for k in range(len(roles)):
+            out = [x for x in opening[p] if x[0] == k]
+            if out:
+
+                @pl.when(role == k)
+                def _(out=out):
+                    for _, link, item in out:
+                        piece_copy(link, item).start()
+
+    for n, p in enumerate(queue):
+        masters[p].wait()
+        array, piece, _, _ = classes[p]
+        height = alls[array].shape[2]
+        master = (value_master, output_master)[array]
+        alls[array][me, piece] = master[piece * height : (piece + 1) * height, :].astype(bf16)
+        if n == len(queue) - 1:
+            for copy in loads:
+                copy.start()
+        if n == 0:
+            pl.semaphore_wait(barrier, 2 + (n_z - 1) + (n_tp - 1))
+        else:
+            open_piece(queue[n - 1])
+    open_piece(queue[-1])
+
     def run_events(k, first, last):
-        events = [e for e in roles[k][0] if first <= e[0] < last]
+        events = [
+            e for e in roles[k][0] if first <= e[0] < last and (e[2] != "send" or e[0] > 0.0)
+        ]
         if not events:
             return
 
@@ -403,8 +478,8 @@
                 (normed, value_factor, input_ref, near_in),
             )
         ):
-            loads[2 + 2 * i].wait()
-            loads[3 + 2 * i].wait()
+            loads[2 * i].wait()
+            loads[2 * i + 1].wait()
             depth = tokens.shape[1]
             rows_here = factor[pl.ds(pl.multiple_of(column * depth, depth), depth), :]
             own[...] = jnp.dot(
@@ -428,7 +503,7 @@
         for k in range(n_tp - 1):
             input_total += near_in[k].astype(f32)
             mixer_total += near_mix[k].astype(f32)
-        for copy in loads[6:8]:
+        for copy in loads[4:6]:
             copy.wait()
         across = (((0,), (0,)), ((), ()))
         for i, (left, right) in enumerate(
@@ -502,7 +577,7 @@
     def moments():
         for copy in b_shares:
             copy.wait_recv()
-        for copy in loads[8:]:
+        for copy in loads[6:]:
             copy.wait()
         for s in range(n_fs):
             wide[s * rows : (s + 1) * rows, :] = shares[s].astype(f32)
@@ -573,41 +648,10 @@
                 step[:, at] = moved
                 new[:, at] = master[:, at] - STEP_RATE * moved
 
-    def copies(level, i, pieces):
-        if pairs:
-            offset = jnp.int32(0)
-            for k in range(len(roles)):
-                offset = jnp.where(role == k, levels_of(n_z, k)[level], offset)
-            source_z = here_z + toward * offset
-        else:
-            offset = jnp.int32(0)
-            for k in range(len(roles)):
-                offset = jnp.where(role == k, levels_of(n_z, k)[level], offset)
-            source_z = here_z + offset
+    def copies(level, i):
+        source_z = level_z(n_z, here_z, level)
         factor = (value_factor, output_factor)[i]
-        out = (value_copy, output_copy)[i]
-        height = alls[i].shape[2]
-        tall = alls[i].shape[1] * height
-        tile = 512 if cols[i] % 512 == 0 else cols[i]
-
-        def body(c, carry):
-            source = source_z * PLANE + c
-            base = pl.multiple_of(source * tall, tall) + pieces[0] * height
-            base = pl.multiple_of(base, height)
-            here = factor[pl.ds(base, len(pieces) * height), :]
-            for t in range(cols[i] // tile):
-                at = slice(t * tile, (t + 1) * tile)
-                inner = slice(starts[i] + t * tile, starts[i] + (t + 1) * tile)
-                moved = jnp.dot(here, high[:, inner], preferred_element_type=f32)
-                for n, p in enumerate(pieces):
-                    old = alls[i][source, p, :, at].astype(f32)
-                    fresh = old - STEP_RATE * moved[n * height : (n + 1) * height]
-                    out[pl.ds(pl.multiple_of(base + n * height, height), height), at] = (
-                        fresh.astype(bf16)
-                    )
-            return carry
-
-        lax.fori_loop(0, PLANE, body, 0)
+        renew(source_z, factor, high, starts[i], alls[i], alls[i], source_z * PLANE)
 
     work = [
         (0.5, products),
@@ -621,24 +665,18 @@
     ]
     free = stages[5] + 0.6
     ready = []
-    for level in range(n_z):
+    for level in range(n_z - 1):
         for i in range(2):
-            count = alls[i].shape[1]
-            groups = [tuple(range(count))]
-            if level == n_z - 1:
-                groups = [(p,) for p in range(count)]
-            for pieces in groups:
-                when = 0.0
-                for k in range(len(roles)):
-                    offset = levels_of(n_z, k)[level]
-                    for item, at in roles[k][1].items():
-                        array, p, _, _ = classes[item[3]]
-                        if item[0] == offset and array == i and p in pieces:
-                            when = max(when, at)
-                ready.append((when, len(ready), level, i, pieces))
-    for when, _, level, i, pieces in sorted(ready):
-        free = max(free + 0.45 * len(pieces) / alls[i].shape[1], when + 0.01)
-        work.append((free, functools.partial(copies, level, i, pieces)))
+            when = 0.0
+            for k in range(len(roles)):
+                offset = levels_of(n_z, k)[level]
+                for at, _, kind, _, item in roles[k][0]:
+                    if item[0] == offset and classes[item[3]][0] == i:
+                        when = max(when, at)
+            ready.append((when, len(ready), level, i))
+    for when, _, level, i in sorted(ready):
+        free = max(free + 0.45, when + 0.01)
+        work.append((free, functools.partial(copies, level, i)))
 
     before = -1.0
     for when, action in sorted(work, key=lambda x: x[0]):
@@ -697,24 +735,29 @@
         output_master,
     )
     outs = []
-    for master, moment in ((value_master, value_moment), (output_master, output_moment)):
+    for master, moment, stack in (
+        (value_master, value_moment, stacks[0]),
+        (output_master, output_moment, stacks[1]),
+    ):
         outs += [
             (master.shape, f32),
             (master.shape, f32),
-            ((n_fs * master.shape[0], master.shape[1]), bf16),
+            (stack, bf16),
             (moment.shape, f32),
             (moment.shape, f32),
         ]
-    return pl.pallas_call(
+    outs += [(value_factor.shape, bf16), (output_factor.shape, bf16), ((rank, both), bf16)]
+    room = (62 << 20) - sum(math.prod(x) * jnp.dtype(t).itemsize for x, t in outs)
+    held = [x for x in streamed if x is not value_factor and x is not output_factor]
+    results = pl.pallas_call(
         functools.partial(step_kernel, n_fs, n_tp),
         out_shape=tuple(pltpu.VMEM(*x) for x in outs),
         in_specs=[pl.BlockSpec(memory_space=pltpu.HBM)] * len(streamed),
         out_specs=(pl.BlockSpec(memory_space=pltpu.VMEM),) * len(outs),
-        scratch_shapes=[pltpu.VMEM(x.shape, x.dtype) for x in streamed]
+        scratch_shapes=[pltpu.VMEM(x.shape, x.dtype) for x in held]
         + [
-            dma((len(streamed),)),
-            pltpu.VMEM(stacks[0], bf16),
-            pltpu.VMEM(stacks[1], bf16),
+            dma((10,)),
+            dma((n_pieces,)),
             pltpu.VMEM((tokens, rank), bf16),
             pltpu.VMEM((tokens, rank), bf16),
             pltpu.VMEM((others, tokens, rank), bf16),
@@ -732,7 +775,6 @@
             pltpu.VMEM((n_fs, rows, both), bf16),
             pltpu.VMEM((rank, both), f32),
             pltpu.VMEM((rank, both), bf16),
-            pltpu.VMEM((rank, both), bf16),
             dma((others, 3)),
             dma((others, 3)),
             dma((n_z + 1,)),
@@ -743,9 +785,60 @@
             dma((n_fs, n_pieces)),
         ],
         compiler_params=pltpu.CompilerParams(
-            collective_id=0, has_side_effects=True, vmem_limit_bytes=39 << 20
+            collective_id=0, has_side_effects=True, vmem_limit_bytes=room
         ),
     )(*streamed)
+    return store(n_fs, results)
+
+
+def store_kernel(n_fs, *refs):
+    results, (value_factor, output_factor, high) = refs[:10], refs[10:13]
+    outs, last, sem = refs[13:23], refs[23:25], refs[25]
+    n_z = n_fs // PLANE
+    here_z = lax.axis_index("fs") // PLANE
+    copies = []
+
+    def begin(src, dst):
+        copy = pltpu.make_async_copy(src, dst, sem.at[len(copies)])
+        copy.start()
+        copies.append(copy)
+
+    for level in range(n_z - 1):
+        at = pl.ds(level_z(n_z, here_z, level) * PLANE, PLANE)
+        for i in (2, 7):
+            begin(results[i].at[at], outs[i].at[at])
+    for i in range(10):
+        if i % 5 != 2:
+            begin(results[i], outs[i])
+    far = level_z(n_z, here_z, n_z - 1)
+    start = 0
+    for i, factor in enumerate((value_factor, output_factor)):
+        old = results[2 + 5 * i]
+        renew(far, factor, high, start, old, last[i], 0)
+        start += old.shape[3]
+        begin(last[i], outs[2 + 5 * i].at[pl.ds(far * PLANE, PLANE)])
+    for copy in copies:
+        copy.wait()
+
+
+def store(n_fs, arrays):
+    outs = [jax.ShapeDtypeStruct(x.shape, x.dtype) for x in arrays[:10]]
+    results = list(
+        pl.pallas_call(
+            functools.partial(store_kernel, n_fs),
+            out_shape=tuple(outs),
+            in_specs=[pl.BlockSpec(memory_space=pltpu.VMEM)] * len(arrays),
+            out_specs=(pl.BlockSpec(memory_space=pltpu.HBM),) * len(outs),
+            scratch_shapes=[
+                pltpu.VMEM((PLANE,) + arrays[i].shape[1:], jnp.bfloat16) for i in (2, 7)
+            ]
+            + [pltpu.SemaphoreType.DMA((2 * (n_fs // PLANE) + 8,))],
+            compiler_params=pltpu.CompilerParams(vmem_limit_bytes=6 << 20),
+        )(*arrays)
+    )
+    for i in (2, 7):
+        results[i] = results[i].reshape(-1, results[i].shape[3])
+    return tuple(results)
 
 
 def solution(mesh):

time: 159 us -> 146 us (0.918)
  local copies, waits for them, and re-layouts: 14.2 us -> 0 us
    unnamed x10 -> x0, local copies, waits for them, and re-layouts: 14.2 us -> none
    pallas_call x0 -> x1, Pallas kernels: none -> 8.23 us  [store(): pl.pallas_call(functools.partial(store_kernel, n_fs), out_shape=tuple(out...]
    pallas_call x1, Pallas kernels: 144 us -> 137 us  [per_device(): pl.pallas_call(functools.partial(step_kernel, n_fs, n_tp), out_shape=tupl...]
where the time goes in v2:
time: 146 us; the launch traced here: 145 us
  Pallas kernels  145 us (99%)
    pallas_call x1, Pallas kernels, per_device(): pl.pallas_call(functools.partial(step_kernel, n_fs, n_tp), out_shape=tupl...  137 us
    pallas_call x1, Pallas kernels, store(): pl.pallas_call(functools.partial(store_kernel, n_fs), out_shape=tuple(out...  8.23 us

profile of v2, /device:TPU:0, one launch (start us, length us, event | category | flops | bytes accessed | tf_op | source)
XLA Modules:
  0.0 145.5 jit_solution(4539220378508500346)
XLA Ops:
  0.6 136.6 %shard_map.195 = (f32[256,1024]{1,0:T(8,128)S(1)}, f32[256,1024]{1,0:T(8,128)S(1)}, bf16[16,4,64,1024]{3,2,1,0:T(8,128)(2,1)S(1)}, f32[128,1024]{1,0:T(8,128)S(1...) custom-call(bf16[512,2048]{1,0:T(8,128)(2,1)} %normed_hbm.1, ...), custom_call_target="tpu_custom_call" | custom-call | tf_op jit(solution)/shard_map/pallas_call | solution.py:752
  137.2 8.2 %shard_map.196 = (f32[256,1024]{1,0:T(8,128)}, f32[256,1024]{1,0:T(8,128)}, bf16[16,4,64,1024]{3,2,1,0:T(8,128)(2,1)}, f32[128,1024]{1,0:T(8,128)}, f32[128,1024...) custom-call(f32[256,1024]{1,0:T(8,128)S(1)} %get-tuple-element.33.re, ...), custom_call_target="tpu_custom_call" | custom-call | tf_op jit(solution)/shard_map/pallas_call | solution.py:827

commit v3 on v2

--- a/solution.py
+++ b/solution.py
@@ -453,15 +453,24 @@
 
     a_sum = message(part.at[pl.ds((1 - here_a) * half, half)], a_recv, across_a, sums, 0)
     b_sum = message(b_part, b_recv, across_b, sums, n_z)
-    z_sums = [
-        message(z_part.at[lax.rem(here_z + k, n_z)], z_recv.at[k], z_mate(k), sums, k)
-        for k in range(1, n_z)
-    ]
+    owners = n_z // 2 if n_z % 4 == 0 else n_z
+    edge = (n_z - owners) // 2
+    depth = n_z // owners
     mine = here_a * half + here_b * n_z
-    z_shares = [
-        message(shares.at[mine + here_z], shares.at[mine + here_z], z_mate(k), shared, k)
-        for k in range(1, n_z)
-    ]
+    is_owner = jnp.logical_and(here_z >= edge, here_z < edge + owners)
+
+    def z_sum(j, k):
+        return message(
+            z_part.at[pl.ds(j * depth, depth)],
+            z_recv.at[k],
+            (edge + j) * PLANE + lax.rem(me, PLANE),
+            sums,
+            k,
+        )
+
+    def z_share(j, k):
+        at = shares.at[pl.ds(mine + j * depth, depth)]
+        return message(at, at, lax.rem(edge + j + k, n_z) * PLANE + lax.rem(me, PLANE), shared, k)
     ours = shares.at[pl.ds(mine, n_z)]
     other = shares.at[pl.ds((1 - here_a) * half + here_b * n_z, n_z)]
     a_share = message(ours, ours, across_a, shared, 0)
@@ -540,21 +549,46 @@
         b_sum.wait_recv()
         quarter[...] += b_recv[...].astype(f32)
         z_part[...] = quarter[...].astype(bf16)
-        start(z_sums)
+        for j in range(owners):
+
+            @pl.when(here_z != edge + j)
+            def _(j=j):
+                z_sum(j, lax.rem(edge + j - here_z + n_z, n_z)).start()
 
     def last_sum():
-        for copy in z_sums:
-            copy.wait_recv()
-        done = quarter[here_z]
-        for k in range(1, n_z):
-            done += z_recv[k].astype(f32)
-        shares[mine + here_z] = done.astype(bf16)
-        start(z_shares)
+        @pl.when(is_owner)
+        def _():
+            j = here_z - edge
+            done = quarter[pl.ds(j * depth, depth)]
+            for k in range(1, n_z):
+                z_sum(j, k).wait_recv()
+                done += z_recv[k].astype(f32)
+            shares[pl.ds(mine + j * depth, depth)] = done.astype(bf16)
+            for k in range(1, n_z):
+                z_share(j, k).start()
 
     def share_a():
-        for copy in z_shares:
-            copy.wait_recv()
+        for j in range(owners):
+
+            @pl.when(here_z != edge + j)
+            def _(j=j):
+                z_share(j, lax.rem(here_z - edge - j + n_z, n_z)).wait_recv()
+
         start([a_share])
+
+    def settle():
+        for copy in pending:
+            copy.wait_send()
+        for j in range(owners):
+
+            @pl.when(here_z != edge + j)
+            def _(j=j):
+                z_sum(j, lax.rem(edge + j - here_z + n_z, n_z)).wait_send()
+
+        @pl.when(is_owner)
+        def _():
+            for k in range(1, n_z):
+                z_share(here_z - edge, k).wait_send()
 
     def share_b():
         a_share.wait_recv()
@@ -686,8 +720,7 @@
         before = when
     for k in range(len(roles)):
         run_events(k, before, float("inf"))
-    for copy in pending:
-        copy.wait_send()
+    settle()
 
 
 def per_device(
@@ -771,7 +804,7 @@
             pltpu.VMEM((n_z, rows, both), bf16),
             pltpu.VMEM((n_z, rows, both), f32),
             pltpu.VMEM((n_z, rows, both), bf16),
-            pltpu.VMEM((n_z, rows, both), bf16),
+            pltpu.VMEM((n_z, 2 if n_z % 4 == 0 else 1, rows, both), bf16),
             pltpu.VMEM((n_fs, rows, both), bf16),
             pltpu.VMEM((rank, both), f32),
             pltpu.VMEM((rank, both), bf16),

time: 146 us -> 144 us (0.986)
  no operation moved by 1% of the time
where the time goes in v3:
time: 144 us
  Pallas kernels  144 us (100%)
    pallas_call x1, Pallas kernels, per_device(): pl.pallas_call(functools.partial(step_kernel, n_fs, n_tp), out_shape=tupl...  135 us
    pallas_call x1, Pallas kernels, store(): pl.pallas_call(functools.partial(store_kernel, n_fs), out_shape=tuple(out...  8.23 us

profile of v3, /device:TPU:0, one launch (start us, length us, event | category | flops | bytes accessed | tf_op | source)
XLA Modules:
  0.0 144.3 jit_solution(17640391362671200416)
XLA Ops:
  0.6 135.4 %shard_map.195 = (f32[256,1024]{1,0:T(8,128)S(1)}, f32[256,1024]{1,0:T(8,128)S(1)}, bf16[16,4,64,1024]{3,2,1,0:T(8,128)(2,1)S(1)}, f32[128,1024]{1,0:T(8,128)S(1...) custom-call(bf16[512,2048]{1,0:T(8,128)(2,1)} %normed_hbm.1, ...), custom_call_target="tpu_custom_call" | custom-call | tf_op jit(solution)/shard_map/pallas_call | solution.py:785
  136.1 8.2 %shard_map.196 = (f32[256,1024]{1,0:T(8,128)}, f32[256,1024]{1,0:T(8,128)}, bf16[16,4,64,1024]{3,2,1,0:T(8,128)(2,1)}, f32[128,1024]{1,0:T(8,128)}, f32[128,1024...) custom-call(f32[256,1024]{1,0:T(8,128)S(1)} %get-tuple-element.33.re, ...), custom_call_target="tpu_custom_call" | custom-call | tf_op jit(solution)/shard_map/pallas_call | solution.py:860

commit v4 on v3

--- a/solution.py
+++ b/solution.py
@@ -18,31 +18,34 @@
 MESH = pl.DeviceIdType.MESH
 A, B, UP, DOWN = range(4)
 PLANE = 4
-GRAIN = 1
-LATENCY = 6
-LEAD = 3.0
-FLIGHT = 1.75
+GRAIN = 4
+LATENCY = 8
+LEAD = 4.0
+FLIGHT = 0.75
 
 
 def pieces_of(rows, cols):
-    count = max(1, min(4 * GRAIN, rows * cols * 2 * GRAIN // 131072))
-    while rows % (16 * count):
-        count -= 1
-    return count
-
-
-def classes_of(counts):
+    if rows % 64 == 0 and rows * cols * 2 >= 4 * 131072:
+        third = rows * 3 // 8 // 16 * 16
+        rest = rows * 3 // 4 - third
+        return [(0, third), (third, rest), (third + rest, rows - third - rest)], 1
+    return [(0, rows)], 0
+
+
+def classes_of(shapes):
     out = []
-    for array, count in enumerate(counts):
-        for p in range(count):
-            plane_first = count % 4 == 0 and p % 4 == 3
-            out.append((array, p, plane_first, A if (p + array) % 2 == 0 else B))
+    for array, shape in enumerate(shapes):
+        ranges, crossing = pieces_of(*shape)
+        for p, (start, height) in enumerate(ranges):
+            plane_first = p >= len(ranges) - crossing
+            flip = A if (p + array) % 2 == 0 else B
+            out.append((array, (start, height), plane_first, flip, height / shape[0]))
     return out
 
 
 def onward(n_z, classes, z, item, via):
     _, fa, fb, p = item
-    _, _, plane_first, order = classes[p]
+    _, _, plane_first, order, _ = classes[p]
     up = [UP] if z < n_z - 1 else []
     down = [DOWN] if z > 0 else []
     if via is None:
@@ -59,7 +62,7 @@
 
 def hops_left(n_z, classes, z, item, link):
     _, fa, fb, p = item
-    _, _, plane_first, order = classes[p]
+    _, _, plane_first, order, _ = classes[p]
     if link in (UP, DOWN):
         return (n_z - 2 - z if link == UP else z - 1) + (0 if plane_first else 2)
     turn = 1 if link == order and (fa, fb) == (0, 0) else 0
@@ -78,6 +81,7 @@
             for link in onward(n_z, classes, z, item, None):
                 pool[z, link].append((0, item))
     missing = n_z * (n_z * PLANE - 1) * len(classes)
+    lengths = [max(1, round(4 * GRAIN * x[4])) for x in classes]
     tick = 0
     while missing:
         for z, item, via in arriving.pop(tick, ()):
@@ -92,7 +96,7 @@
                     if way == link and start * GRAIN == tick
                 ]
                 if held:
-                    busy[z, link] = tick + held[0]
+                    busy[z, link] = max(tick, busy[z, link]) + held[0]
                 waiting = pool[z, link]
                 if busy[z, link] > tick or not waiting:
                     continue
@@ -119,8 +123,8 @@
                 else:
                     there, got = z + (1 if link == UP else -1), item
                 takes[there].append((tick, link, got))
-                arriving[tick + LATENCY * GRAIN].append((there, got, link))
-                busy[z, link] = tick + 1
+                arriving[tick + lengths[p] + (LATENCY - 1) * GRAIN].append((there, got, link))
+                busy[z, link] = tick + lengths[p]
                 missing -= 1
         tick += 1
     return sends, takes
@@ -133,7 +137,7 @@
     )
 
 
-def roles_of(n_z, sends, takes):
+def roles_of(n_z, classes, sends, takes):
     pairs = n_z % 2 == 0 and all(
         sorted(x[z]) == mirrored(n_z, x[n_z - 1 - z])
         for x in (sends, takes)
@@ -145,7 +149,7 @@
         done = {}
         for tick, link, (source, fa, fb, p) in sorted(takes[z]):
             item = (source - z, fa, fb, p)
-            done[item] = tick / GRAIN + FLIGHT
+            done[item] = tick / GRAIN + 4 * classes[p][4] + FLIGHT
             events.append((done[item], 0, "take", link, item))
         last = collections.defaultdict(float)
         for tick, link, (source, fa, fb, p) in sorted(sends[z]):
@@ -178,8 +182,7 @@
 
 
 def renew(source_z, factor, high, start, old, out, first):
-    _, count, height, cols = old.shape
-    tall = count * height
+    _, tall, cols = old.shape
     tile = 512 if cols % 512 == 0 else cols
 
     def body(c, carry):
@@ -189,12 +192,8 @@
             at = slice(t * tile, (t + 1) * tile)
             inner = slice(start + t * tile, start + (t + 1) * tile)
             moved = jnp.dot(here, high[:, inner], preferred_element_type=jnp.float32)
-            for p in range(count):
-                fresh = (
-                    old[source, p, :, at].astype(jnp.float32)
-                    - STEP_RATE * moved[p * height : (p + 1) * height]
-                )
-                out[first + c, p, :, at] = fresh.astype(jnp.bfloat16)
+            fresh = old[source, :, at].astype(jnp.float32) - STEP_RATE * moved
+            out[first + c, :, at] = fresh.astype(jnp.bfloat16)
         return carry
 
     lax.fori_loop(0, PLANE, body, 0)
@@ -278,8 +277,8 @@
     rows = total.shape[1]
     cols = (value_cot.shape[1], output_cot.shape[1])
     starts = (0, cols[0])
-    classes = classes_of([x.shape[1] for x in alls])
-    fine = len(classes) == 8 * GRAIN
+    classes = classes_of([x.shape[1:] for x in alls])
+    fine = len(classes) == 6
 
     if fine:
         reserved = (
@@ -297,7 +296,7 @@
         reserved = ()
         stages = tuple(7.8 + 4 * i for i in range(6))
     sends, takes = plan(n_z, classes, reserved)
-    pairs, roles = roles_of(n_z, sends, takes)
+    pairs, roles = roles_of(n_z, classes, sends, takes)
     if pairs:
         toward = jnp.where(2 * here_z < n_z, 1, -1)
         role = jnp.where(2 * here_z < n_z, here_z, n_z - 1 - here_z)
@@ -323,10 +322,9 @@
         return lax.rem(here_z + k, n_z) * PLANE + lax.rem(me, PLANE)
 
     masters = []
-    for array, p, _, _ in classes:
+    for array, (first, height), _, _, _ in classes:
         hbm, master = ((value_master_hbm, value_master), (output_master_hbm, output_master))[array]
-        height = alls[array].shape[2]
-        at = pl.ds(p * height, height)
+        at = pl.ds(first, height)
         masters.append(
             pltpu.make_async_copy(hbm.at[at], master.at[at], master_sem.at[len(masters)])
         )
@@ -376,8 +374,8 @@
     def piece_copy(link, item):
         offset, fa, fb, p = item
         source = (here_z + toward * offset) * PLANE + places[fa, fb]
-        array, piece, _, _ = classes[p]
-        there = alls[array].at[source, piece]
+        array, (first, height), _, _, _ = classes[p]
+        there = alls[array].at[source, pl.ds(first, height)]
         return pltpu.make_async_remote_copy(
             src_ref=there,
             dst_ref=there,
@@ -399,10 +397,10 @@
 
     for n, p in enumerate(queue):
         masters[p].wait()
-        array, piece, _, _ = classes[p]
-        height = alls[array].shape[2]
+        array, (first, height), _, _, _ = classes[p]
+        at = slice(first, first + height)
         master = (value_master, output_master)[array]
-        alls[array][me, piece] = master[piece * height : (piece + 1) * height, :].astype(bf16)
+        alls[array][me, at, :] = master[at, :].astype(bf16)
         if n == len(queue) - 1:
             for copy in loads:
                 copy.start()
@@ -696,6 +694,7 @@
         (stages[4], share_b),
         (stages[5], moments),
         (stages[5] + 0.5, steps),
+        (stages[5] + 4.0, settle),
     ]
     free = stages[5] + 0.6
     ready = []
@@ -720,7 +719,6 @@
         before = when
     for k in range(len(roles)):
         run_events(k, before, float("inf"))
-    settle()
 
 
 def per_device(
@@ -750,9 +748,8 @@
     dma = pltpu.SemaphoreType.DMA
     stacks = []
     for master in (value_master, output_master):
-        count = pieces_of(*master.shape)
-        stacks.append((n_fs, count, master.shape[0] // count, master.shape[1]))
-    n_pieces = stacks[0][1] + stacks[1][1]
+        stacks.append((n_fs,) + master.shape)
+    n_pieces = len(classes_of([x[1:] for x in stacks]))
     streamed = (
         normed_input,
         mixer_output,
@@ -848,7 +845,7 @@
     for i, factor in enumerate((value_factor, output_factor)):
         old = results[2 + 5 * i]
         renew(far, factor, high, start, old, last[i], 0)
-        start += old.shape[3]
+        start += old.shape[2]
         begin(last[i], outs[2 + 5 * i].at[pl.ds(far * PLANE, PLANE)])
     for copy in copies:
         copy.wait()
@@ -870,7 +867,7 @@
         )(*arrays)
     )
     for i in (2, 7):
-        results[i] = results[i].reshape(-1, results[i].shape[3])
+        results[i] = results[i].reshape(-1, results[i].shape[2])
     return tuple(results)
 
 

time: 144 us -> 143 us (level)
  Pallas kernels: 144 us -> 142 us
    pallas_call x1, Pallas kernels: 135 us -> 134 us  [per_device(): pl.pallas_call(functools.partial(step_kernel, n_fs, n_tp), out_shape=tupl...]
where the time goes in v4:
time: 143 us
  Pallas kernels  142 us (99%)
    pallas_call x1, Pallas kernels, per_device(): pl.pallas_call(functools.partial(step_kernel, n_fs, n_tp), out_shape=tupl...  134 us
    pallas_call x1, Pallas kernels, store(): pl.pallas_call(functools.partial(store_kernel, n_fs), out_shape=tuple(out...  8.23 us

profile of v4, /device:TPU:0, one launch (start us, length us, event | category | flops | bytes accessed | tf_op | source)
XLA Modules:
  0.0 142.9 jit_solution(16706583348557865952)
XLA Ops:
  0.6 134.0 %shard_map.195 = (f32[256,1024]{1,0:T(8,128)S(1)}, f32[256,1024]{1,0:T(8,128)S(1)}, bf16[16,256,1024]{2,1,0:T(8,128)(2,1)S(1)}, f32[128,1024]{1,0:T(8,128)S(1)},...) custom-call(bf16[512,2048]{1,0:T(8,128)(2,1)} %normed_hbm.1, ...), custom_call_target="tpu_custom_call" | custom-call | tf_op jit(solution)/shard_map/pallas_call | solution.py:782
  134.6 8.2 %shard_map.196 = (f32[256,1024]{1,0:T(8,128)}, f32[256,1024]{1,0:T(8,128)}, bf16[16,256,1024]{2,1,0:T(8,128)(2,1)}, f32[128,1024]{1,0:T(8,128)}, f32[128,1024]{1...) custom-call(f32[256,1024]{1,0:T(8,128)S(1)} %get-tuple-element.33.re, ...), custom_call_target="tpu_custom_call" | custom-call | tf_op jit(solution)/shard_map/pallas_call | solution.py:857
